TPU v7x, 256 devices: a whole 4x4x8 slice. The times are simulated.
256 devices in a mesh: sp: 64 (over z, x, core), tp: 4 (over y).
Axes of the slice: x: 4, y: 4, z: 8, core: 2. Of those that a mesh axis runs over, the one named last changes fastest.
Arguments:
- stream: bfloat16 [8192, 2048], P(('sp', 'tp')), may hold values from -2.5 to 2.5
- recurrence_input: bfloat16 [8192, 2, 1024], P('sp', None, 'tp'), may hold values from -6 to 6
- output_gate_input: bfloat16 [8192, 2, 1024], P('sp', None, 'tp'), may hold values from -6 to 6
- convolution_taps: bfloat16 [4, 2, 1024], P(None, None, 'tp'), may hold values from -4 to 4
- first_group_gates: bfloat16 [2, 16, 64, 64], P(None, 'tp'), may hold values from -0.75 to 0.75
- second_group_gates: bfloat16 [2, 8, 128, 128], P(None, 'tp'), may hold values from -0.5 to 0.5
- channel_decay: float32 [2, 1024], P(None, 'tp'), may hold values from 4.7 to 13.6
- position_log_extra: float32 [8192, 2, 1024], P('sp', None, 'tp'), may hold values from -1.4 to 0, as said below
- recurrence_output_weight: bfloat16 [2, 1024, 2048], P(None, 'tp'), may hold values from -0.125 to 0.125
- first_norm_gain: float32 [2048], replicated, may hold values from 0.1 to 1.9
- first_norm_bias: float32 [2048], replicated, may hold values from -1.75 to 1.75
- routed_expert_index: int32 [8192, 4], P('sp'), may hold values from 0 to 63, all different within a row; in each aligned block of 32 rows (0 to 31, 32 to 63, ...) at most 2 rows name the same one
- routed_expert_weight: float32 [8192, 4], P('sp'), may hold values from 0.25 to 1
- routed_gate_weight: bfloat16 [64, 2048, 512], P('sp', None, 'tp'), may hold values from -0.125 to 0.125
- routed_up_weight: bfloat16 [64, 2048, 512], P('sp', None, 'tp'), may hold values from -0.125 to 0.125
- routed_down_weight: bfloat16 [64, 512, 2048], P('sp', 'tp'), may hold values from -0.25 to 0.25
- shared_gate_weight: bfloat16 [2048, 512], replicated, may hold values from -0.125 to 0.125
- shared_up_weight: bfloat16 [2048, 512], replicated, may hold values from -0.125 to 0.125
- shared_down_weight: bfloat16 [512, 2048], replicated, may hold values from -0.25 to 0.25
- second_norm_gain: float32 [2048], replicated, may hold values from 0.1 to 1.9
- second_norm_bias: float32 [2048], replicated, may hold values from -1.75 to 1.75
Outputs:
- result: bfloat16 [8192, 2048], P(('sp', 'tp'))
Inputs may be any that keep to these rules, and one draw needn't show every extreme that they name: `routed_expert_index`: each row names 4 different experts. In each aligned block of 32 rows no expert is named more than 2 times, and in some block an expert is named exactly 2 times. `position_log_extra`: every entry is negative.
All inputs are finite; a program needn't handle non-finite values.
Results may differ from a plain program's by a relative error of at most 0.015.
Values may be sent and summed in bfloat16 or wider, within the bound.
A program may use at most 64 MiB of HBM per device.

v0:
```python
import jax
import jax.numpy as jnp
from jax import lax
from jax.sharding import PartitionSpec as P

RESIDUAL_SCALE = 8.0**0.25
NORM_EPSILON = 1e-05


def copy_for_each(shard, axis):
    count = lax.axis_size(axis)
    return lax.all_to_all(
        jnp.broadcast_to(shard[None], (count, *shard.shape)), axis, 0, 0, tiled=True
    )


def all_in_one(shard, axis):
    leaves = jax.tree.leaves(shard)
    sequence = sorted(range(len(leaves)), key=lambda k: -leaves[k].size)
    width = (1, *leaves[sequence[0]].shape)[-1]
    lines = [
        jnp.pad(leaves[k].reshape(-1), (0, -leaves[k].size % width)).reshape(-1, width)
        for k in sequence
    ]
    both, at, found = (copy_for_each(jnp.concatenate(lines), axis), 0, {})
    for k, line in zip(sequence, lines):
        slab = both[:, at : at + len(line)].reshape(len(both), -1)
        found[k] = slab[:, : leaves[k].size].reshape(-1, *leaves[k].shape)
        at += len(line)
    numbers = iter(range(len(leaves)))
    return jax.tree.map(lambda _: found[next(numbers)], shard)


def joined_by_halves(pieces, combine):
    while len(jax.tree.leaves(pieces)[0]) > 1:
        pieces = jax.vmap(combine)(
            *(jax.tree.map(lambda part: part[side::2], pieces) for side in (0, 1))
        )
    return jax.tree.map(lambda part: part[0], pieces)


def entering(shard, axis, combine, identity):
    count, mine = (lax.axis_size(axis), lax.axis_index(axis))
    passed = jnp.arange(count) < mine

    def kept(part, zero, own):
        part = jnp.where(
            passed.reshape(-1, *(1 for _ in own.shape)), part, jnp.asarray(zero, own.dtype)
        )
        return part

    pieces = all_in_one(shard, axis)
    return joined_by_halves(jax.tree.map(kept, pieces, identity, shard), combine)


def shifted(shard, axis, by):
    count = lax.axis_size(axis)
    pairs = [(i, i + by) for i in range(count) if 0 <= i + by < count]
    return lax.ppermute(shard, axis, pairs)


def cut_along(shard, dim, count):
    dims = shard.shape
    pieces = shard.reshape(*dims[:dim], count, dims[dim] // count, *dims[dim + 1 :])
    return jnp.moveaxis(pieces, dim, 0)


def summed_on_arrival(shard, axis, dim):
    count = lax.axis_size(axis)
    pieces = lax.all_to_all(cut_along(shard, dim, count), axis, 0, 0, tiled=True)
    return jnp.sum(pieces.astype(jnp.float32), axis=0)


def layer_norm(values, gain_vec, bias_vec):
    row_mean = jnp.mean(values, axis=-1, keepdims=True)
    spread = jnp.mean(jnp.square(values - row_mean), axis=-1, keepdims=True)
    return (values - row_mean) * lax.rsqrt(spread + NORM_EPSILON) * gain_vec + bias_vec


def block_gates(conv_rows, weights, head_size):
    length = conv_rows.shape[0]
    head_rows = conv_rows.reshape(length, -1, head_size)
    pre_act = jnp.einsum("thc,ghcd->gthd", head_rows, weights, preferred_element_type=jnp.float32)
    gate_pair = jax.nn.sigmoid(pre_act).reshape(2, length, -1)
    return (gate_pair[0], gate_pair[1])


def chain_link(first_part, second_part):
    return (first_part[0] * second_part[0], second_part[0] * first_part[1] + second_part[1])


def carried(totals):
    unity = jnp.ones_like(totals[0])
    nought = jnp.zeros_like(totals[1])
    return entering(totals, "sp", chain_link, (unity, nought))[1]


def expert_terms(picked, letters, gate_w, up_w, down_w):
    gate_form = letters + "d,ldf->" + letters + "f"
    down_form = letters + "f,lfd->" + letters + "d"
    gated = jnp.einsum(gate_form, picked, gate_w, preferred_element_type=jnp.float32)
    lifted = jnp.einsum(gate_form, picked, up_w, preferred_element_type=jnp.float32)
    hidden = (jax.nn.silu(gated) * lifted).astype(jnp.bfloat16)
    return jnp.einsum(down_form, hidden, down_w, preferred_element_type=jnp.float32)


def shards(
    stream,
    recurrence_input,
    output_gate_input,
    convolution_taps,
    first_group_gates,
    second_group_gates,
    channel_decay,
    position_log_extra,
    recurrence_output_weight,
    first_norm_gain,
    first_norm_bias,
    routed_expert_index,
    routed_expert_weight,
    routed_gate_weight,
    routed_up_weight,
    routed_down_weight,
    shared_gate_weight,
    shared_up_weight,
    shared_down_weight,
    second_norm_gain,
    second_norm_bias,
):
    length = recurrence_input.shape[0]
    tap_count = convolution_taps.shape[0]
    border = shifted(recurrence_input[length - (tap_count - 1) :], "sp", 1)
    padded = jnp.concatenate([border, recurrence_input], axis=0).astype(jnp.float32)
    tap_weights = convolution_taps.astype(jnp.float32)
    summed = tap_weights[0] * padded[0:length]
    for offset in range(1, tap_count):
        summed = summed + tap_weights[offset] * padded[offset : offset + length]
    conv_rows = summed.astype(jnp.bfloat16)
    recur_a, input_a = block_gates(conv_rows[:, 0], first_group_gates, first_group_gates.shape[-1])
    recur_b, input_b = block_gates(
        conv_rows[:, 1], second_group_gates, second_group_gates.shape[-1]
    )
    recurrence_gate = jnp.stack([recur_a, recur_b], axis=1)
    input_gate = jnp.stack([input_a, input_b], axis=1)
    decay_logarithm = -8.0 * recurrence_gate * jax.nn.softplus(-channel_decay) + position_log_extra
    decay_rate = jnp.exp(decay_logarithm)
    driving = (
        jnp.sqrt(-jnp.expm1(2.0 * decay_logarithm)) * input_gate * conv_rows.astype(jnp.float32)
    )
    running = jnp.cumsum(decay_logarithm, axis=0)
    tail_sum = jnp.sum(jnp.exp(running[-1] - running) * driving, axis=0)
    incoming = carried((jnp.exp(running[-1]), tail_sum))
    opening = driving[:1] + decay_rate[:1] * incoming
    started = jnp.concatenate([opening, driving[1:]], axis=0)
    states = lax.associative_scan(chain_link, (decay_rate, started), axis=0)[1]
    branch_output = (jax.nn.gelu(output_gate_input.astype(jnp.float32)) * states).astype(
        jnp.bfloat16
    )
    tp_count = lax.axis_size("tp")
    quarter = length // tp_count
    mixed = summed_on_arrival(
        jnp.einsum(
            "tgc,gcd->td",
            branch_output,
            recurrence_output_weight,
            preferred_element_type=jnp.float32,
        ).astype(jnp.bfloat16),
        "tp",
        0,
    )
    normed = layer_norm(
        RESIDUAL_SCALE * stream.astype(jnp.float32) + mixed, first_norm_gain, first_norm_bias
    ).astype(jnp.bfloat16)
    width = normed.shape[1]
    top_count = routed_expert_index.shape[1]
    local_count = routed_gate_weight.shape[0]
    expert_count = local_count * lax.axis_size("sp")
    capacity = max(2, 5 * quarter * top_count // (4 * expert_count))
    block_ids = routed_expert_index.reshape(tp_count, quarter * top_count)
    onehot = (
        block_ids[:, :, None] == jnp.arange(expert_count, dtype=jnp.int32)[None, None, :]
    ).astype(jnp.int32)
    slot_ranks = jnp.sum((jnp.cumsum(onehot, axis=1) - onehot) * onehot, axis=2)
    own_index = lax.axis_index("tp")
    own_ids = lax.dynamic_index_in_dim(block_ids, own_index, 0, keepdims=False)
    own_ranks = lax.dynamic_index_in_dim(slot_ranks, own_index, 0, keepdims=False)
    blank_row = jnp.zeros((1, width), jnp.bfloat16)
    padded_rows = jnp.concatenate([normed, blank_row], axis=0)
    targets = own_ids * capacity + own_ranks
    sources = jnp.arange(quarter * top_count, dtype=jnp.int32) // top_count
    table = jnp.full((expert_count * capacity,), quarter, jnp.int32).at[targets].set(sources)
    outgoing = jnp.take(padded_rows, table, axis=0).reshape(expert_count, capacity, width)
    arrived = lax.all_to_all(outgoing, "sp", split_axis=0, concat_axis=0, tiled=True)
    slots = arrived.shape[1]
    fanned = lax.all_gather(arrived[None], "tp", axis=0, tiled=True)
    shaped = fanned.reshape(tp_count, -1, local_count, slots, width)
    partial_value = expert_terms(
        shaped, "xslc", routed_gate_weight, routed_up_weight, routed_down_weight
    )
    summed_rows = summed_on_arrival(partial_value.astype(jnp.bfloat16), "tp", 0)
    leaving = summed_rows.astype(jnp.bfloat16).reshape(-1, slots, width)
    returned = lax.all_to_all(leaving, "sp", split_axis=0, concat_axis=0, tiled=True)
    picked_rows = returned.reshape(expert_count * capacity, width)[own_ids * capacity + own_ranks]
    own_weights = lax.dynamic_slice_in_dim(routed_expert_weight, own_index * quarter, quarter, 0)
    routed = jnp.sum(
        own_weights[:, :, None]
        * picked_rows.reshape(quarter, top_count, width).astype(jnp.float32),
        axis=1,
    )
    shared_hidden = (
        jax.nn.silu(jnp.dot(normed, shared_gate_weight, preferred_element_type=jnp.float32))
        * jnp.dot(normed, shared_up_weight, preferred_element_type=jnp.float32)
    ).astype(jnp.bfloat16)
    shared_out = jnp.dot(shared_hidden, shared_down_weight, preferred_element_type=jnp.float32)
    final = layer_norm(
        RESIDUAL_SCALE * normed.astype(jnp.float32) + (shared_out + routed),
        second_norm_gain,
        second_norm_bias,
    )
    return final.astype(jnp.bfloat16)


def solution(mesh):
    in_specs = (
        P(("sp", "tp"), None),
        P("sp", None, "tp"),
        P("sp", None, "tp"),
        P(None, None, "tp"),
        P(None, "tp", None, None),
        P(None, "tp", None, None),
        P(None, "tp"),
        P("sp", None, "tp"),
        P(None, "tp", None),
        P(),
        P(),
        P("sp", None),
        P("sp", None),
        P("sp", None, "tp"),
        P("sp", None, "tp"),
        P("sp", "tp", None),
        P(),
        P(),
        P(),
        P(),
        P(),
    )
    out_specs = P(("sp", "tp"), None)
    return jax.shard_map(shards, mesh=mesh, in_specs=in_specs, out_specs=out_specs, check_vma=False)
```

profile of v0, /device:TPU:1, one launch (start us, length us, event | category | flops | bytes accessed | tf_op | source)
XLA Modules:
  0.0 205.7 jit_solution(793034132163294517)
XLA Ops:
  6.5 1.1 copy.130
  7.6 4.5 %collective-permute-start = (bf16[3,2,256]{2,0,1:T(4,128)(2,1)S(1)}, bf16[3,2,256]{2,0,1:T(4,128)(2,1)S(1)}, u32[]{:S(2)}, u32[]{:S(2)}) collective-permute-start(bf16[3,2,256]{2,0,1:T(4,128)(2,1)S(1)} %slice.395), channel_id=1, source_target_pairs={{0,4},{4,8},{8,12},{12,16},{16,20},{20,24},{24,28},{28,32},{32,36}... | collective-permute-start | bytes 9224 | tf_op jit(solution)/shard_map/ppermute | solution.py:59
  12.1 0.7 convert_element_type.67
  12.9 0.7 fusion.84
  13.6 0.8 copy.147
  14.4 0.7 reshape.136
  15.1 0.1 fusion.45
  15.2 0.1 copy.132
  15.4 0.3 fusion.20
  15.7 0.1 copy.138
  15.8 0.1 copy.134
  16.0 0.3 fusion.16
  16.3 0.1 copy.165
  16.4 1.0 fusion.101
  17.4 0.2 fusion.53
  17.6 0.6 slice_bitcast_fusion
  18.1 0.6 fusion.99
  18.7 0.1 copy.141
  18.8 0.8 copy.166
  19.6 1.2 fusion.52
  20.9 0.7 broadcast_in_dim.61
  21.6 11.3 %all-to-all-start = ((f32[64,4,256]{2,1,0:T(4,128)}), f32[64,4,256]{2,1,0:T(4,128)S(1)}, u32[]{:S(2)}, u32[]{:S(2)}) async-start(f32[64,4,256]{2,1,0:T(4,128)} %broadcast_in_dim.61), calls=%async_computation | async-start | bytes 524288 | tf_op jit(solution)/shard_map/all_to_all | solution.py:12
  32.9 0.8 fusion.60
  33.7 0.3 reduce_window_sum.23
  34.0 0.9 select_reduce_fusion
  34.9 0.7 fusion.90
  35.6 1.5 scatter_custom_fusion
  37.1 0.7 slice.345
  37.9 0.7 slice.343
  38.7 7.3 %all-to-all-done = f32[64,4,256]{2,1,0:T(4,128)S(1)} async-done(((f32[64,4,256]{2,1,0:T(4,128)}), f32[64,4,256]{2,1,0:T(4,128)S(1)}, u32[]{:S(2)}, u32[]{:S(2)}) %all-to-all-start) | async-done | bytes 262176 | tf_op jit(solution)/shard_map/all_to_all | solution.py:12
  46.0 0.1 fusion.103
  46.2 0.6 slice.315
  46.8 0.6 slice.316
  47.5 0.9 fusion.109
  49.0 1.0 fusion.106
  51.7 1.3 fusion.1
  53.0 4.3 %all-to-all-start.1 = ((bf16[4,32,2048]{2,1,0:T(8,128)(2,1)}), bf16[4,32,2048]{2,1,0:T(8,128)(2,1)S(1)}, u32[]{:S(2)}, u32[]{:S(2)}) async-start(bf16[4,32,2048]{2,1,0:T(8,128)(2,1)} %bitcast.17), calls=%async_computation.1 | async-start | bytes 1048576 | tf_op jit(solution)/shard_map/all_to_all | solution.py:70
  57.3 0.1 broadcast_in_dim.65
  57.5 8.8 %all-to-all-done.1 = bf16[4,32,2048]{2,1,0:T(8,128)(2,1)S(1)} async-done(((bf16[4,32,2048]{2,1,0:T(8,128)(2,1)}), bf16[4,32,2048]{2,1,0:T(8,128)(2,1)S(1)}, u32[]{:S(2)}, u32[]{:S(2)}) %all-to-all-start.1) | async-done | bytes 524320 | tf_op jit(solution)/shard_map/all_to_all | solution.py:70
  66.4 0.2 fusion.71
  66.6 0.2 multiply_reduce_fusion.2
  66.8 0.1 add_convert_fusion.1
  67.0 0.9 gather_fusion
  67.9 1.1 gather.10
  69.0 1.6 broadcast_select_fusion
  70.6 23.1 %all_to_all.25 = bf16[64,2,2048]{2,1,0:T(2,128)(2,1)S(1)} all-to-all(bf16[64,2,2048]{2,1,0:T(2,128)(2,1)S(1)} %broadcast_select_fusion), channel_id=1, replica_groups=mesh['sp'=64,'tp'=4] {'sp'}, dimensions={0} | all-to-all | bytes 1048576 | tf_op jit(solution)/shard_map/all_to_all | solution.py:193
  93.8 1.0 copy.148
  94.8 27.8 %all-gather.3.cloned.1.call-done = bf16[256,2,2048]{2,0,1:T(8,128)(2,1)} async-done(((bf16[64,2,2048]{2,0,1:T(8,128)(2,1)}), bf16[256,2,2048]{2,0,1:T(8,128)(2,1)}) %all-gather.3.cloned.1.call-update) | async-done | bytes 2097168 | tf_op jit(solution)/shard_map/all_gather | solution.py:195
  122.6 2.4 %fusion.7 = f32[4,64,1,2,128]{4,1,3,0,2:T(8,128)S(1)} fusion(bf16[4,64,2,2048]{3,1,0,2:T(8,128)(2,1)} %bitcast.118, bf16[1,2048,128]{2,1,0:T(8,128)(2,1)} %param.34), kind=kOutput, calls=%fused_computation.14 | convolution fusion | flops 268435456 | bytes 2883584 | tf_op jit(solution)/shard_map/xslcd,ldf->xslcf/dot_general | solution.py:101
  125.0 5.2 %fusion = bf16[4,1,64,1,2,2048]{5,2,4,3,1,0:T(8,128)(2,1)} fusion(bf16[4,64,2,2048]{3,1,0,2:T(8,128)(2,1)} %bitcast.119, bf16[1,128,2048]{2,1,0:T(8,128)(2,1)S(1)} %copy-done.2, bf16[1,2048,128]{2,1,0:T(8,128)(2,1)S(1)} %copy-done.3, f32[4,64,1,2,128]{4,1,3,0,2:T(8,128)S(1)} %fusion.7), kind=kOutput, calls=%fused_computation.4 | convolution fusion | flops 538312704 | bytes 5505024 | tf_op jit(solution)/shard_map/xslcf,lfd->xslcd/dot_general | solution.py:104
  130.2 28.9 %all_to_all.26 = bf16[4,1,64,1,2,2048]{5,2,4,3,1,0:T(8,128)(2,1)S(1)} all-to-all(bf16[4,1,64,1,2,2048]{5,2,4,3,1,0:T(8,128)(2,1)} %fusion), channel_id=1, replica_groups=mesh['sp'=64,'tp'=4] {'tp'}, dimensions={0} | all-to-all | bytes 4194304 | tf_op jit(solution)/shard_map/all_to_all | solution.py:70
  159.2 0.4 bitcast_reduce_fusion
  159.5 1.3 copy.153
  160.9 11.9 %all-to-all-start.4 = ((bf16[64,2,2048]{2,1,0:T(2,128)(2,1)}), bf16[64,2,2048]{2,1,0:T(2,128)(2,1)S(1)}, u32[]{:S(2)}, u32[]{:S(2)}) async-start(bf16[64,2,2048]{2,1,0:T(2,128)(2,1)} %copy.153), calls=%async_computation.4 | async-start | bytes 1048576 | tf_op jit(solution)/shard_map/all_to_all | solution.py:202
  172.9 0.1 copy.146
  173.0 2.7 %fusion.118 = f32[32,512]{1,0:T(8,128)} fusion(bf16[32,2048]{1,0:T(8,128)(2,1)S(1)} %add_convert_fusion.1, bf16[2048,512]{1,0:T(8,128)(2,1)} %param.37), kind=kOutput, calls=%fused_computation.192 | convolution fusion | flops 67108864 | bytes 2293760 | tf_op jit(solution)/shard_map/dot_general | solution.py:211
  175.6 14.8 %all-to-all-done.4 = bf16[64,2,2048]{2,1,0:T(2,128)(2,1)S(1)} async-done(((bf16[64,2,2048]{2,1,0:T(2,128)(2,1)}), bf16[64,2,2048]{2,1,0:T(2,128)(2,1)S(1)}, u32[]{:S(2)}, u32[]{:S(2)}) %all-to-all-start.4) | async-done | bytes 524320 | tf_op jit(solution)/shard_map/all_to_all | solution.py:202
  190.5 0.2 reshape.142
  190.7 1.7 gather_fusion.1
  192.4 1.4 reshape.143
  193.8 0.7 multiply_reduce_fusion
  194.5 3.3 %fusion.117 = (f32[32]{0:T(128)S(1)}, f32[32,2048]{1,0:T(8,128)S(1)}) fusion(f32[32,2048]{1,0:T(8,128)S(1)} %multiply_reduce_fusion, bf16[512,2048]{1,0:T(8,128)(2,1)} %param.39, bf16[32,2048]{1,0:T(8,128)(2,1)S(1)} %add_convert_fusion.1, bf16[2048,512]{1,0:T(8,128)(2,1)} %param.38, f32[32,512]{1,0:T(8,128)} %fusion.118), kind=kOutput, calls=%fused_computation.191 | convolution fusion | flops 134643680 | bytes 4915328 | tf_op jit(solution)/shard_map/dot_general | solution.py:214
  197.8 0.2 multiply_reduce_fusion.1
  198.0 0.8 add_convert_fusion
  (165 shorter events, 2.6 us)
Async XLA Ops:
  6.5 45.1 %copy-start = (bf16[2,256,2048]{2,1,0:T(8,128)(2,1)S(1)}, bf16[2,256,2048]{2,1,0:T(8,128)(2,1)}, u32[]{:S(2)}) copy-start(bf16[2,256,2048]{2,1,0:T(8,128)(2,1)} %param.29) | copy-start | bytes 6291460
  6.5 8.9 %copy-start.19 = (bf16[2,4,64,64]{3,2,1,0:T(8,128)(2,1)S(1)}, bf16[2,4,64,64]{3,2,1,0:T(8,128)(2,1)}, u32[]{:S(2)}) copy-start(bf16[2,4,64,64]{3,2,1,0:T(8,128)(2,1)} %param.25) | copy-start | bytes 196612
  7.6 7.4 %collective-permute-start = (bf16[3,2,256]{2,0,1:T(4,128)(2,1)S(1)}, bf16[3,2,256]{2,0,1:T(4,128)(2,1)S(1)}, u32[]{:S(2)}, u32[]{:S(2)}) collective-permute-start(bf16[3,2,256]{2,0,1:T(4,128)(2,1)S(1)} %slice.395), channel_id=1, source_target_pairs={{0,4},{4,8},{8,12},{12,16},{16,20},{20,24},{24,28},{28,32},{32,36}... | collective-permute-start | bytes 9224 | tf_op jit(solution)/shard_map/ppermute | solution.py:59
  12.8 2.5 %copy-start.7 = (f32[2,256]{1,0:T(2,128)}, f32[2,256]{1,0:T(2,128)S(1)}, u32[]{:S(2)}) copy-start(f32[2,256]{1,0:T(2,128)S(1)} %get-tuple-element.37) | copy-start | bytes 6148
  12.8 2.5 %copy-start.8 = (f32[2,256]{1,0:T(2,128)}, f32[2,256]{1,0:T(2,128)S(1)}, u32[]{:S(2)}) copy-start(f32[2,256]{1,0:T(2,128)S(1)} %get-tuple-element.38) | copy-start | bytes 6148
  12.8 2.5 %copy-start.9 = (f32[2,256]{1,0:T(2,128)}, f32[2,256]{1,0:T(2,128)S(1)}, u32[]{:S(2)}) copy-start(f32[2,256]{1,0:T(2,128)S(1)} %get-tuple-element.39) | copy-start | bytes 6148
  12.9 2.5 %copy-start.10 = (f32[2,256]{1,0:T(2,128)}, f32[2,256]{1,0:T(2,128)S(1)}, u32[]{:S(2)}) copy-start(f32[2,256]{1,0:T(2,128)S(1)} %get-tuple-element.40) | copy-start | bytes 6148
  15.0 0.9 copy-start.20
  19.6 1.2 copy-start.15
  21.6 24.4 %all-to-all-start = ((f32[64,4,256]{2,1,0:T(4,128)}), f32[64,4,256]{2,1,0:T(4,128)S(1)}, u32[]{:S(2)}, u32[]{:S(2)}) async-start(f32[64,4,256]{2,1,0:T(4,128)} %broadcast_in_dim.61), calls=%async_computation | async-start | bytes 524288 | tf_op jit(solution)/shard_map/all_to_all | solution.py:12
  35.6 12.9 %copy-start.17 = (s32[128]{0:T(128)}, s32[128]{0:T(128)S(1)}, u32[]{:S(2)}) copy-start(s32[128]{0:T(128)S(1)} %fusion.90) | copy-start | bytes 1540
  48.9 1.2 copy-start.5
  50.3 1.2 copy-start.6
  50.8 0.9 copy-start.4
  51.7 5.6 %copy-start.21 = (s32[128]{0:T(128)S(1)}, s32[128]{0:T(128)}, u32[]{:S(2)}) copy-start(s32[128]{0:T(128)} %scatter_custom_fusion) | copy-start | bytes 1540
  51.7 14.7 %copy-start.1 = (bf16[32,2048]{1,0:T(8,128)(2,1)S(1)}, bf16[32,2048]{1,0:T(8,128)(2,1)}, u32[]{:S(2)}) copy-start(bf16[32,2048]{1,0:T(8,128)(2,1)} %param.21) | copy-start | bytes 393220
  53.0 13.8 %copy-start.11 = (f32[2048]{0:T(1024)S(1)}, f32[2048]{0:T(1024)}, u32[]{:S(2)}) copy-start(f32[2048]{0:T(1024)} %param.31) | copy-start | bytes 24580
  53.0 13.8 %copy-start.12 = (f32[2048]{0:T(1024)S(1)}, f32[2048]{0:T(1024)}, u32[]{:S(2)}) copy-start(f32[2048]{0:T(1024)} %param.30) | copy-start | bytes 24580
  53.0 13.3 %all-to-all-start.1 = ((bf16[4,32,2048]{2,1,0:T(8,128)(2,1)}), bf16[4,32,2048]{2,1,0:T(8,128)(2,1)S(1)}, u32[]{:S(2)}, u32[]{:S(2)}) async-start(bf16[4,32,2048]{2,1,0:T(8,128)(2,1)} %bitcast.17), calls=%async_computation.1 | async-start | bytes 1048576 | tf_op jit(solution)/shard_map/all_to_all | solution.py:70
  57.3 65.3 %all-gather.3.cloned.1.call-start = ((), (), s32[]{:S(2)}) async-start(), calls=%async_computation.5 | async-start | bytes 2621440 | tf_op jit(solution)/shard_map/all_gather | solution.py:195
  94.7 30.2 %copy-start.2 = (bf16[1,128,2048]{2,1,0:T(8,128)(2,1)S(1)}, bf16[1,128,2048]{2,1,0:T(8,128)(2,1)}, u32[]{:S(2)}) copy-start(bf16[1,128,2048]{2,1,0:T(8,128)(2,1)} %param.36) | copy-start | bytes 1572868
  94.7 30.2 %copy-start.3 = (bf16[1,2048,128]{2,1,0:T(8,128)(2,1)S(1)}, bf16[1,2048,128]{2,1,0:T(8,128)(2,1)}, u32[]{:S(2)}) copy-start(bf16[1,2048,128]{2,1,0:T(8,128)(2,1)} %param.35) | copy-start | bytes 1572868
  159.2 13.6 %copy-start.16 = (f32[128,4]{0,1:T(4,128)S(1)}, f32[128,4]{0,1:T(4,128)}, u32[]{:S(2)}) copy-start(f32[128,4]{0,1:T(4,128)} %param.33) | copy-start | bytes 6148
  159.2 13.8 %copy-start.18 = (s32[128]{0:T(128)S(1)}, s32[128]{0:T(128)}, u32[]{:S(2)}) copy-start(s32[128]{0:T(128)} %copy-done.17) | copy-start | bytes 1540
  160.9 29.6 %all-to-all-start.4 = ((bf16[64,2,2048]{2,1,0:T(2,128)(2,1)}), bf16[64,2,2048]{2,1,0:T(2,128)(2,1)S(1)}, u32[]{:S(2)}, u32[]{:S(2)}) async-start(bf16[64,2,2048]{2,1,0:T(2,128)(2,1)} %copy.153), calls=%async_computation.4 | async-start | bytes 1048576 | tf_op jit(solution)/shard_map/all_to_all | solution.py:202
  194.5 3.5 %copy-start.13 = (f32[2048]{0:T(1024)S(1)}, f32[2048]{0:T(1024)}, u32[]{:S(2)}) copy-start(f32[2048]{0:T(1024)} %param.41) | copy-start | bytes 24580
  194.5 3.5 %copy-start.14 = (f32[2048]{0:T(1024)S(1)}, f32[2048]{0:T(1024)}, u32[]{:S(2)}) copy-start(f32[2048]{0:T(1024)} %param.40) | copy-start | bytes 24580
Sparse Core Ops, SparseCore 0:
  94.9 27.6 all-gather.2
where the time goes:
time: 207 us; the launch traced here: 206 us
  waiting for transfers between devices  58.8 us (28%)
  blocking collectives  52.1 us (25%)
  starting transfers between devices  32 us (15%)
  local copies, waits for them, and re-layouts  19.8 us (10%)
  matrix products  15.4 us (7%)
  between operations  14.3 us (7%)
  other arithmetic  13.3 us (6%)
    all_to_all x1, blocking collectives, summed_on_arrival(): lax.all_to_all(cut_along(shard, dim, count), axis, 0, 0, tiled=True)  28.9 us
    all_gather x1, waiting for transfers between devices, shards(): fanned = lax.all_gather(arrived[None], 'tp', axis=0, tiled=True)  27.8 us
    all_to_all x1, blocking collectives, shards(): lax.all_to_all(outgoing, 'sp', split_axis=0, concat_axis=0, tiled=True)  23.1 us
    all_to_all x1, waiting for transfers between devices, shards(): lax.all_to_all(leaving, 'sp', split_axis=0, concat_axis=0, tiled=True)  14.8 us
    all_to_all x1, starting transfers between devices, shards(): lax.all_to_all(leaving, 'sp', split_axis=0, concat_axis=0, tiled=True)  11.9 us
    all_to_all x1, starting transfers between devices, copy_for_each(): lax.all_to_all(jnp.broadcast_to(shard[None], (count, *shard.shape)), axis...  11.3 us
    all_to_all x1, waiting for transfers between devices, summed_on_arrival(): lax.all_to_all(cut_along(shard, dim, count), axis, 0, 0, tiled=True)  8.83 us
    all_to_all x1, waiting for transfers between devices, copy_for_each(): lax.all_to_all(jnp.broadcast_to(shard[None], (count, *shard.shape)), axis...  7.34 us
  transfers between devices with their start and end apart: 5, of which 4 were waited for; matrix products, arithmetic and copies ran while one was open for 6% of the time, Pallas kernels for 0%

commit v1 on v0

--- a/solution.py
+++ b/solution.py
@@ -5,6 +5,12 @@
 
 RESIDUAL_SCALE = 8.0**0.25
 NORM_EPSILON = 1e-05
+
+
+def record_watch(in_array):
+    local_next = jnp.stack([in_array for _ in range(lax.axis_size("tp"))], 0)
+    t1 = lax.all_to_all(local_next, "tp", split_axis=0, concat_axis=0)
+    return jnp.concatenate(t1, axis=0)
 
 
 def copy_for_each(shard, axis):
@@ -192,7 +198,7 @@
     outgoing = jnp.take(padded_rows, table, axis=0).reshape(expert_count, capacity, width)
     arrived = lax.all_to_all(outgoing, "sp", split_axis=0, concat_axis=0, tiled=True)
     slots = arrived.shape[1]
-    fanned = lax.all_gather(arrived[None], "tp", axis=0, tiled=True)
+    fanned = record_watch(arrived[None])
     shaped = fanned.reshape(tp_count, -1, local_count, slots, width)
     partial_value = expert_terms(
         shaped, "xslc", routed_gate_weight, routed_up_weight, routed_down_weight

time: 207 us -> 188 us (0.908)
  blocking collectives: 52.1 us -> 80.5 us
  waiting for transfers between devices: 58.8 us -> 31.1 us
  between operations: 14.3 us -> 0.87 us
  starting transfers between devices: 32 us -> 27.2 us
    all_to_all x0 -> x1, blocking collectives: none -> 28.6 us  [record_watch(): t1 = lax.all_to_all(local_next, 'tp', split_axis=0, concat_axis=0)]
    all_gather x1 -> x0, waiting for transfers between devices: 27.8 us -> none  [shards(): fanned = lax.all_gather(arrived[None], 'tp', axis=0, tiled=True)]
    all_to_all x1, starting transfers between devices: 11.9 us -> 7.11 us  [shards(): lax.all_to_all(leaving, 'sp', split_axis=0, concat_axis=0, tiled=True)]
  transfers between devices with their start and end apart: 5 -> 4, of which waited for: 4 -> 3; matrix products, arithmetic and copies ran while one was open for 6% -> 6% of each run, Pallas kernels for 0% -> 0%
where the time goes in v1:
time: 188 us; the launch traced here: 187 us
  blocking collectives  80.5 us (43%)
  waiting for transfers between devices  31.1 us (17%)
  starting transfers between devices  27.2 us (14%)
  local copies, waits for them, and re-layouts  20.5 us (11%)
  matrix products  14 us (7%)
  other arithmetic  13.3 us (7%)
    all_to_all x1, blocking collectives, summed_on_arrival(): lax.all_to_all(cut_along(shard, dim, count), axis, 0, 0, tiled=True)  28.8 us
    all_to_all x1, blocking collectives, record_watch(): t1 = lax.all_to_all(local_next, 'tp', split_axis=0, concat_axis=0)  28.6 us
    all_to_all x1, blocking collectives, shards(): lax.all_to_all(outgoing, 'sp', split_axis=0, concat_axis=0, tiled=True)  23.1 us
    all_to_all x1, waiting for transfers between devices, shards(): lax.all_to_all(leaving, 'sp', split_axis=0, concat_axis=0, tiled=True)  14.8 us
    all_to_all x1, starting transfers between devices, copy_for_each(): lax.all_to_all(jnp.broadcast_to(shard[None], (count, *shard.shape)), axis...  11.3 us
    all_to_all x1, waiting for transfers between devices, summed_on_arrival(): lax.all_to_all(cut_along(shard, dim, count), axis, 0, 0, tiled=True)  8.84 us
    all_to_all x1, waiting for transfers between devices, copy_for_each(): lax.all_to_all(jnp.broadcast_to(shard[None], (count, *shard.shape)), axis...  7.4 us
    all_to_all x1, starting transfers between devices, shards(): lax.all_to_all(leaving, 'sp', split_axis=0, concat_axis=0, tiled=True)  7.11 us
  transfers between devices with their start and end apart: 4, of which 3 were waited for; matrix products, arithmetic and copies ran while one was open for 6% of the time, Pallas kernels for 0%

profile of v1, /device:TPU:1, one launch (start us, length us, event | category | flops | bytes accessed | tf_op | source)
XLA Modules:
  0.0 187.5 jit_solution(10463653834387888441)
XLA Ops:
  0.0 1.1 copy.122
  1.1 4.5 %collective-permute-start = (bf16[3,2,256]{2,0,1:T(4,128)(2,1)S(1)}, bf16[3,2,256]{2,0,1:T(4,128)(2,1)S(1)}, u32[]{:S(2)}, u32[]{:S(2)}) collective-permute-start(bf16[3,2,256]{2,0,1:T(4,128)(2,1)S(1)} %slice.395), channel_id=1, source_target_pairs={{0,4},{4,8},{8,12},{12,16},{16,20},{20,24},{24,28},{28,32},{32,36}... | collective-permute-start | bytes 9224 | tf_op jit(solution)/shard_map/ppermute | solution.py:65
  5.6 0.7 convert_element_type.67
  6.3 0.7 fusion.84
  7.0 0.8 copy.139
  7.8 0.7 reshape.139
  8.5 0.1 fusion.45
  8.7 0.1 copy.124
  8.9 0.3 fusion.20
  9.2 0.1 copy.130
  9.3 0.1 copy.126
  9.4 0.3 fusion.16
  9.7 0.1 copy.155
  9.8 1.0 fusion.101
  10.8 0.2 fusion.53
  11.0 0.6 slice_bitcast_fusion
  11.6 0.6 fusion.99
  12.3 0.8 copy.156
  13.1 1.2 fusion.52
  14.4 0.7 broadcast_in_dim.58
  15.1 11.3 %all-to-all-start = ((f32[64,4,256]{2,1,0:T(4,128)}), f32[64,4,256]{2,1,0:T(4,128)S(1)}, u32[]{:S(2)}, u32[]{:S(2)}) async-start(f32[64,4,256]{2,1,0:T(4,128)} %broadcast_in_dim.58), calls=%async_computation | async-start | bytes 524288 | tf_op jit(solution)/shard_map/all_to_all | solution.py:18
  26.4 0.8 fusion.60
  27.3 0.3 reduce_window_sum.23
  27.5 0.9 select_reduce_fusion
  28.4 0.7 fusion.90
  29.1 1.4 scatter_custom_fusion
  30.6 0.7 slice.345
  31.3 0.7 slice.343
  32.1 7.4 %all-to-all-done = f32[64,4,256]{2,1,0:T(4,128)S(1)} async-done(((f32[64,4,256]{2,1,0:T(4,128)}), f32[64,4,256]{2,1,0:T(4,128)S(1)}, u32[]{:S(2)}, u32[]{:S(2)}) %all-to-all-start) | async-done | bytes 262176 | tf_op jit(solution)/shard_map/all_to_all | solution.py:18
  39.5 0.1 fusion.103
  39.7 0.6 slice.315
  40.4 0.7 slice.316
  41.1 0.9 fusion.109
  42.5 1.0 fusion.106
  45.2 1.3 fusion.1
  46.5 4.3 %all-to-all-start.1 = ((bf16[4,32,2048]{2,1,0:T(8,128)(2,1)}), bf16[4,32,2048]{2,1,0:T(8,128)(2,1)S(1)}, u32[]{:S(2)}, u32[]{:S(2)}) async-start(bf16[4,32,2048]{2,1,0:T(8,128)(2,1)} %bitcast.17), calls=%async_computation.1 | async-start | bytes 1048576 | tf_op jit(solution)/shard_map/all_to_all | solution.py:76
  50.8 0.1 broadcast_in_dim.62
  51.0 8.8 %all-to-all-done.1 = bf16[4,32,2048]{2,1,0:T(8,128)(2,1)S(1)} async-done(((bf16[4,32,2048]{2,1,0:T(8,128)(2,1)}), bf16[4,32,2048]{2,1,0:T(8,128)(2,1)S(1)}, u32[]{:S(2)}, u32[]{:S(2)}) %all-to-all-start.1) | async-done | bytes 524320 | tf_op jit(solution)/shard_map/all_to_all | solution.py:76
  60.0 0.2 fusion.71
  60.1 0.2 multiply_reduce_fusion.2
  60.3 0.1 add_convert_fusion.1
  60.5 0.9 gather_fusion
  61.4 1.1 gather.10
  62.6 1.6 broadcast_select_fusion
  64.2 23.1 %all_to_all.30 = bf16[64,2,2048]{2,1,0:T(2,128)(2,1)S(1)} all-to-all(bf16[64,2,2048]{2,1,0:T(2,128)(2,1)S(1)} %broadcast_select_fusion), channel_id=1, replica_groups=mesh['sp'=64,'tp'=4] {'sp'}, dimensions={0} | all-to-all | bytes 1048576 | tf_op jit(solution)/shard_map/all_to_all | solution.py:199
  87.3 0.2 copy.140
  87.4 0.2 stack.11
  87.7 28.6 %all_to_all.31 = bf16[4,1,64,2,2048]{4,2,3,1,0:T(8,128)(2,1)S(1)} all-to-all(bf16[4,1,64,2,2048]{4,2,3,1,0:T(8,128)(2,1)S(1)} %stack.11), channel_id=1, replica_groups=mesh['sp'=64,'tp'=4] {'tp'}, dimensions={0} | all-to-all | bytes 4194304 | tf_op jit(solution)/shard_map/all_to_all | solution.py:12
  116.4 1.3 copy-done.1
  117.7 0.7 fusion.7
  118.4 5.5 %fusion = bf16[4,1,64,1,2,2048]{5,2,4,3,1,0:T(8,128)(2,1)} fusion(bf16[4,1,64,2,2048]{4,2,3,1,0:T(8,128)(2,1)} %copy-done.1, bf16[1,128,2048]{2,1,0:T(8,128)(2,1)} %param.36, bf16[1,2048,128]{2,1,0:T(8,128)(2,1)} %param.35, f32[4,64,1,2,128]{4,1,3,0,2:T(8,128)S(1)} %fusion.7), kind=kOutput, calls=%fused_computation.4 | convolution fusion | flops 538312704 | bytes 5505024 | tf_op jit(solution)/shard_map/xslcf,lfd->xslcd/dot_general | solution.py:110
  123.9 28.8 %all_to_all.32 = bf16[4,1,64,1,2,2048]{5,2,4,3,1,0:T(8,128)(2,1)S(1)} all-to-all(bf16[4,1,64,1,2,2048]{5,2,4,3,1,0:T(8,128)(2,1)} %fusion), channel_id=1, replica_groups=mesh['sp'=64,'tp'=4] {'tp'}, dimensions={0} | all-to-all | bytes 4194304 | tf_op jit(solution)/shard_map/all_to_all | solution.py:76
  152.6 0.4 bitcast_reduce_fusion
  153.0 1.3 copy.143
  154.3 7.1 %all-to-all-start.5 = ((bf16[64,2,2048]{2,1,0:T(2,128)(2,1)}), bf16[64,2,2048]{2,1,0:T(2,128)(2,1)S(1)}, u32[]{:S(2)}, u32[]{:S(2)}) async-start(bf16[64,2,2048]{2,1,0:T(2,128)(2,1)} %copy.143), calls=%async_computation.5 | async-start | bytes 1048576 | tf_op jit(solution)/shard_map/all_to_all | solution.py:208
  161.6 2.7 %fusion.118 = f32[32,512]{1,0:T(8,128)} fusion(bf16[32,2048]{1,0:T(8,128)(2,1)S(1)} %add_convert_fusion.1, bf16[2048,512]{1,0:T(8,128)(2,1)} %param.37), kind=kOutput, calls=%fused_computation.192 | convolution fusion | flops 67108864 | bytes 2293760 | tf_op jit(solution)/shard_map/dot_general | solution.py:217
  164.3 14.8 %all-to-all-done.5 = bf16[64,2,2048]{2,1,0:T(2,128)(2,1)S(1)} async-done(((bf16[64,2,2048]{2,1,0:T(2,128)(2,1)}), bf16[64,2,2048]{2,1,0:T(2,128)(2,1)S(1)}, u32[]{:S(2)}, u32[]{:S(2)}) %all-to-all-start.5) | async-done | bytes 524320 | tf_op jit(solution)/shard_map/all_to_all | solution.py:208
  179.1 0.2 reshape.146
  179.3 1.7 gather_fusion.1
  181.1 1.4 reshape.147
  182.4 0.7 multiply_reduce_fusion
  183.2 3.3 %fusion.117 = (f32[32]{0:T(128)S(1)}, f32[32,2048]{1,0:T(8,128)S(1)}) fusion(f32[32,2048]{1,0:T(8,128)S(1)} %multiply_reduce_fusion, bf16[512,2048]{1,0:T(8,128)(2,1)} %param.39, bf16[32,2048]{1,0:T(8,128)(2,1)S(1)} %add_convert_fusion.1, bf16[2048,512]{1,0:T(8,128)(2,1)} %param.38, f32[32,512]{1,0:T(8,128)} %fusion.118), kind=kOutput, calls=%fused_computation.191 | convolution fusion | flops 134643680 | bytes 4915328 | tf_op jit(solution)/shard_map/dot_general | solution.py:220
  186.5 0.2 multiply_reduce_fusion.1
  186.7 0.8 add_convert_fusion
  (164 shorter events, 2.7 us)
Async XLA Ops:
  0.0 45.2 %copy-start = (bf16[2,256,2048]{2,1,0:T(8,128)(2,1)S(1)}, bf16[2,256,2048]{2,1,0:T(8,128)(2,1)}, u32[]{:S(2)}) copy-start(bf16[2,256,2048]{2,1,0:T(8,128)(2,1)} %param.29) | copy-start | bytes 6291460
  0.0 8.9 %copy-start.19 = (bf16[2,4,64,64]{3,2,1,0:T(8,128)(2,1)S(1)}, bf16[2,4,64,64]{3,2,1,0:T(8,128)(2,1)}, u32[]{:S(2)}) copy-start(bf16[2,4,64,64]{3,2,1,0:T(8,128)(2,1)} %param.25) | copy-start | bytes 196612
  1.1 7.4 %collective-permute-start = (bf16[3,2,256]{2,0,1:T(4,128)(2,1)S(1)}, bf16[3,2,256]{2,0,1:T(4,128)(2,1)S(1)}, u32[]{:S(2)}, u32[]{:S(2)}) collective-permute-start(bf16[3,2,256]{2,0,1:T(4,128)(2,1)S(1)} %slice.395), channel_id=1, source_target_pairs={{0,4},{4,8},{8,12},{12,16},{16,20},{20,24},{24,28},{28,32},{32,36}... | collective-permute-start | bytes 9224 | tf_op jit(solution)/shard_map/ppermute | solution.py:65
  6.3 2.5 %copy-start.7 = (f32[2,256]{1,0:T(2,128)}, f32[2,256]{1,0:T(2,128)S(1)}, u32[]{:S(2)}) copy-start(f32[2,256]{1,0:T(2,128)S(1)} %get-tuple-element.37) | copy-start | bytes 6148
  6.3 2.5 %copy-start.8 = (f32[2,256]{1,0:T(2,128)}, f32[2,256]{1,0:T(2,128)S(1)}, u32[]{:S(2)}) copy-start(f32[2,256]{1,0:T(2,128)S(1)} %get-tuple-element.38) | copy-start | bytes 6148
  6.3 2.5 %copy-start.9 = (f32[2,256]{1,0:T(2,128)}, f32[2,256]{1,0:T(2,128)S(1)}, u32[]{:S(2)}) copy-start(f32[2,256]{1,0:T(2,128)S(1)} %get-tuple-element.39) | copy-start | bytes 6148
  6.3 2.5 %copy-start.10 = (f32[2,256]{1,0:T(2,128)}, f32[2,256]{1,0:T(2,128)S(1)}, u32[]{:S(2)}) copy-start(f32[2,256]{1,0:T(2,128)S(1)} %get-tuple-element.40) | copy-start | bytes 6148
  8.5 0.9 copy-start.20
  13.1 1.2 copy-start.15
  15.1 24.4 %all-to-all-start = ((f32[64,4,256]{2,1,0:T(4,128)}), f32[64,4,256]{2,1,0:T(4,128)S(1)}, u32[]{:S(2)}, u32[]{:S(2)}) async-start(f32[64,4,256]{2,1,0:T(4,128)} %broadcast_in_dim.58), calls=%async_computation | async-start | bytes 524288 | tf_op jit(solution)/shard_map/all_to_all | solution.py:18
  29.1 13.0 %copy-start.17 = (s32[128]{0:T(128)}, s32[128]{0:T(128)S(1)}, u32[]{:S(2)}) copy-start(s32[128]{0:T(128)S(1)} %fusion.90) | copy-start | bytes 1540
  42.4 1.2 copy-start.5
  43.8 1.2 copy-start.6
  44.3 0.9 copy-start.4
  45.2 5.6 %copy-start.21 = (s32[128]{0:T(128)S(1)}, s32[128]{0:T(128)}, u32[]{:S(2)}) copy-start(s32[128]{0:T(128)} %scatter_custom_fusion) | copy-start | bytes 1540
  45.2 14.7 %copy-start.2 = (bf16[32,2048]{1,0:T(8,128)(2,1)S(1)}, bf16[32,2048]{1,0:T(8,128)(2,1)}, u32[]{:S(2)}) copy-start(bf16[32,2048]{1,0:T(8,128)(2,1)} %param.21) | copy-start | bytes 393220
  46.5 13.8 %copy-start.11 = (f32[2048]{0:T(1024)S(1)}, f32[2048]{0:T(1024)}, u32[]{:S(2)}) copy-start(f32[2048]{0:T(1024)} %param.31) | copy-start | bytes 24580
  46.5 13.8 %copy-start.12 = (f32[2048]{0:T(1024)S(1)}, f32[2048]{0:T(1024)}, u32[]{:S(2)}) copy-start(f32[2048]{0:T(1024)} %param.30) | copy-start | bytes 24580
  46.5 13.3 %all-to-all-start.1 = ((bf16[4,32,2048]{2,1,0:T(8,128)(2,1)}), bf16[4,32,2048]{2,1,0:T(8,128)(2,1)S(1)}, u32[]{:S(2)}, u32[]{:S(2)}) async-start(bf16[4,32,2048]{2,1,0:T(8,128)(2,1)} %bitcast.17), calls=%async_computation.1 | async-start | bytes 1048576 | tf_op jit(solution)/shard_map/all_to_all | solution.py:76
  87.7 30.0 %copy-start.3 = (bf16[1,2048,128]{2,1,0:T(8,128)(2,1)S(1)}, bf16[1,2048,128]{2,1,0:T(8,128)(2,1)}, u32[]{:S(2)}) copy-start(bf16[1,2048,128]{2,1,0:T(8,128)(2,1)} %param.34) | copy-start | bytes 1572868
  116.3 1.3 copy-start.1
  152.6 8.8 %copy-start.16 = (f32[128,4]{0,1:T(4,128)S(1)}, f32[128,4]{0,1:T(4,128)}, u32[]{:S(2)}) copy-start(f32[128,4]{0,1:T(4,128)} %param.33) | copy-start | bytes 6148
  152.6 9.0 %copy-start.18 = (s32[128]{0:T(128)S(1)}, s32[128]{0:T(128)}, u32[]{:S(2)}) copy-start(s32[128]{0:T(128)} %copy-done.17) | copy-start | bytes 1540
  154.3 24.8 %all-to-all-start.5 = ((bf16[64,2,2048]{2,1,0:T(2,128)(2,1)}), bf16[64,2,2048]{2,1,0:T(2,128)(2,1)S(1)}, u32[]{:S(2)}, u32[]{:S(2)}) async-start(bf16[64,2,2048]{2,1,0:T(2,128)(2,1)} %copy.143), calls=%async_computation.5 | async-start | bytes 1048576 | tf_op jit(solution)/shard_map/all_to_all | solution.py:208
  183.2 3.5 %copy-start.13 = (f32[2048]{0:T(1024)S(1)}, f32[2048]{0:T(1024)}, u32[]{:S(2)}) copy-start(f32[2048]{0:T(1024)} %param.41) | copy-start | bytes 24580
  183.2 3.5 %copy-start.14 = (f32[2048]{0:T(1024)S(1)}, f32[2048]{0:T(1024)}, u32[]{:S(2)}) copy-start(f32[2048]{0:T(1024)} %param.40) | copy-start | bytes 24580
